TPU v7x, 32 devices: a whole 2x2x4 slice. The times are simulated.
32 devices in a mesh: sp: 4 (over z), tp: 4 (over y, x), dp: 2 (over core).
Axes of the slice: x: 2, y: 2, z: 4, core: 2. Of those that a mesh axis runs over, the one named last changes fastest.
Arguments:
- latent_tokens: bfloat16 [4096, 2048], P(('dp', 'sp', 'tp')), parts along dimension 0, may hold values from -6 to 6
- condition: bfloat16 [4096], P(('dp', 'sp')), parts along dimension 0, may hold values from -6 to 6
- shift_weight: bfloat16 [2048, 2048], P('sp', 'tp'), may hold values from -0.125 to 0.125
- scale_weight: bfloat16 [2048, 2048], P('sp', 'tp'), may hold values from -0.125 to 0.125
- gate_weight: bfloat16 [2048, 2048], P('sp', 'tp'), may hold values from -0.125 to 0.125
- norm_gain: float32 [2048], replicated, may hold values from 0.1 to 1.9
- query_down: bfloat16 [2048, 512], replicated, may hold values from -0.125 to 0.125
- query_gain: float32 [512], replicated, may hold values from 0.1 to 1.9
- kv_down: bfloat16 [2048, 256], replicated, may hold values from -0.125 to 0.125
- kv_gain: float32 [256], replicated, may hold values from 0.1 to 1.9
- rope_down: bfloat16 [2048, 32], replicated, may hold values from -0.125 to 0.125
- query_up: bfloat16 [512, 1536], P(None, 'tp'), may hold values from -0.25 to 0.25
- key_up: bfloat16 [256, 1024], P(None, 'tp'), may hold values from -0.375 to 0.375
- value_up: bfloat16 [256, 1024], P(None, 'tp'), may hold values from -0.375 to 0.375
- query_norm_gain: float32 [96], replicated, may hold values from 0.47 to 16
- key_norm_gain: float32 [96], replicated, may hold values from 0.47 to 16
- out_weight: bfloat16 [1024, 2048], P('tp'), may hold values from -0.1875 to 0.1875
- context_latent: bfloat16 [2048, 256], P(('dp', 'sp')), parts along dimension 0, may hold values from -6 to 6
- context_rope: bfloat16 [2048, 32], P(('dp', 'sp')), parts along dimension 0, may hold values from -6 to 6
- context_lift: float32 [16], P('tp'), may hold values from 0 to 2
Outputs:
- output: bfloat16 [4096, 2048], P(('dp', 'sp', 'tp')), parts along dimension 0
There are 2 independent parts, one for each index of `dp`. A program takes and returns all parts, laid end to end along the dimension named above; an argument that names none is the same for every part. Nothing has to cross between parts.
All inputs are finite; a program needn't handle non-finite values.
Results may differ from a plain program's by a relative error of at most 0.015.
The roundings to bfloat16 on the way count: a program that leaves them out, or rounds other values in their place, can miss the bound.
Values may be sent and summed in bfloat16 or wider, within the bound.
A program may use at most 128 MiB of HBM per device.

v0:
```python
import jax
import jax.numpy as jnp
from jax import lax
from jax.sharding import PartitionSpec as P

NOPE_DIM = 64
ROPE_DIM = 32
VALUE_DIM = 64
QK_DIM = 96
GRID_W = 64


EPS = 1e-06
THETA = 10000.0


def rms_scaled(values, gain_vector):
    mean_square = jnp.mean(values * values, axis=-1, keepdims=True)
    return values * lax.rsqrt(mean_square + EPS) * gain_vector


def rotate(rope_part, positions):
    row_count = rope_part.shape[0]
    freq_count = ROPE_DIM // 4
    inverse = THETA ** (-4.0 * jnp.arange(freq_count, dtype=jnp.float32) / ROPE_DIM)
    grid_row = (positions // GRID_W).astype(jnp.float32)
    grid_col = (positions % GRID_W).astype(jnp.float32)
    angles = jnp.stack([grid_row[:, None] * inverse, grid_col[:, None] * inverse], axis=1)
    cosine_table = jnp.cos(angles)[:, None]
    sine_table = jnp.sin(angles)[:, None]
    split_rows = rope_part.reshape(row_count, rope_part.shape[1], 2, 2, freq_count)
    first_half = split_rows[:, :, :, 0]
    second_half = split_rows[:, :, :, 1]
    turned = jnp.stack(
        [
            first_half * cosine_table - second_half * sine_table,
            second_half * cosine_table + first_half * sine_table,
        ],
        axis=3,
    )
    return turned.reshape(rope_part.shape)


def build_keys(
    latent_rows, rope_rows, first_index, shard_rows, group_rows, key_up, value_up, key_norm_gain
):
    row_count = latent_rows.shape[0]
    head_count = key_up.shape[1] // NOPE_DIM
    nope_part = jnp.dot(latent_rows, key_up, preferred_element_type=jnp.float32).reshape(
        row_count, head_count, NOPE_DIM
    )
    value_rows = jnp.dot(latent_rows, value_up, preferred_element_type=jnp.float32).astype(
        jnp.bfloat16
    )
    shared = jnp.broadcast_to(
        rope_rows.astype(jnp.float32)[:, None, :], (row_count, head_count, ROPE_DIM)
    )
    normal_keys = rms_scaled(jnp.concatenate([nope_part, shared], axis=-1), key_norm_gain)
    row_index = first_index + jnp.arange(row_count, dtype=jnp.int32)
    within = row_index % shard_rows
    is_latent = within < group_rows
    positions = row_index // shard_rows * group_rows + within
    turned = rotate(normal_keys[..., NOPE_DIM:], positions)
    rope_part = jnp.where(is_latent[:, None, None], turned, normal_keys[..., NOPE_DIM:])
    key_rows = jnp.concatenate([normal_keys[..., :NOPE_DIM], rope_part], axis=-1).astype(
        jnp.bfloat16
    )
    return (key_rows.reshape(row_count, head_count * QK_DIM), value_rows)


def key_offset(first_index, row_count, shard_rows, group_rows, context_lift):
    row_index = first_index + jnp.arange(row_count, dtype=jnp.int32)
    is_context = row_index % shard_rows >= group_rows
    return jnp.where(is_context[None, :], context_lift[:, None], jnp.zeros((), jnp.float32))


def attend_block(carried, queries, key_rows, value_rows, offset):
    running_max, weight_sum, accumulated = carried
    row_count = key_rows.shape[0]
    head_count = queries.shape[1]
    key_heads = key_rows.reshape(row_count, head_count, QK_DIM)
    value_heads = value_rows.reshape(row_count, head_count, VALUE_DIM)
    scores = jnp.einsum(
        "qhd,khd->hqk", queries, key_heads, preferred_element_type=jnp.float32
    ) * QK_DIM ** (-0.5)
    scores = scores + offset[:, None, :]
    new_max = jnp.maximum(running_max, jnp.max(scores, axis=-1))
    factor = jnp.exp(running_max - new_max)
    weights = jnp.exp(scores - new_max[..., None])
    weight_sum = weight_sum * factor + jnp.sum(weights, axis=-1)
    product = jnp.einsum(
        "hqk,khd->qhd",
        weights.astype(jnp.bfloat16),
        value_heads,
        preferred_element_type=jnp.float32,
    )
    accumulated = accumulated * factor.T[:, :, None] + product
    return (new_max, weight_sum, accumulated)


def fold_blocks(carried, pieces, shard_rows, block_step):
    block_count = pieces[0].shape[0] // shard_rows
    blocked = tuple(
        (
            piece_rows.reshape((block_count, shard_rows) + piece_rows.shape[1:])
            for piece_rows in pieces
        )
    )
    starts = shard_rows * jnp.arange(block_count, dtype=jnp.int32)

    def one_block(state_now, inputs):
        return (block_step(state_now, inputs[:-1], inputs[-1]), None)

    final_state, ignored = lax.scan(one_block, carried, blocked + (starts,))
    return final_state


def local(
    latent_tokens,
    condition,
    shift_weight,
    scale_weight,
    gate_weight,
    norm_gain,
    query_down,
    query_gain,
    kv_down,
    kv_gain,
    rope_down,
    query_up,
    key_up,
    value_up,
    query_norm_gain,
    key_norm_gain,
    out_weight,
    context_latent,
    context_rope,
    context_lift,
):
    activated = jax.nn.silu(condition.astype(jnp.float32)).astype(jnp.bfloat16)[None]
    shift_term = jnp.dot(activated, shift_weight, preferred_element_type=jnp.float32)[0]
    scale_term = jnp.dot(activated, scale_weight, preferred_element_type=jnp.float32)[0]
    gate_term = jnp.dot(activated, gate_weight, preferred_element_type=jnp.float32)[0]
    shift_sum, scale_sum, gate_sum = lax.psum((shift_term, scale_term, gate_term), "sp")
    mod_shift, mod_scale, mod_gate = (
        lax.all_gather(shift_sum, "tp", axis=0, tiled=True),
        lax.all_gather(scale_sum, "tp", axis=0, tiled=True),
        lax.all_gather(gate_sum, "tp", axis=0, tiled=True),
    )
    token_values = latent_tokens.astype(jnp.float32)
    normed = (rms_scaled(token_values, norm_gain) * (1.0 + mod_scale) + mod_shift).astype(
        jnp.bfloat16
    )
    query_latent = rms_scaled(
        jnp.dot(normed, query_down, preferred_element_type=jnp.float32), query_gain
    ).astype(jnp.bfloat16)
    key_latent = rms_scaled(
        jnp.dot(normed, kv_down, preferred_element_type=jnp.float32), kv_gain
    ).astype(jnp.bfloat16)
    rope_key = jnp.dot(normed, rope_down, preferred_element_type=jnp.float32).astype(jnp.bfloat16)
    query_group, latent_group, rope_group = (
        lax.all_gather(query_latent, "tp", axis=0, tiled=True),
        lax.all_gather(key_latent, "tp", axis=0, tiled=True),
        lax.all_gather(rope_key, "tp", axis=0, tiled=True),
    )
    group_rows = query_group.shape[0]
    head_count = query_up.shape[1] // QK_DIM
    positions = lax.axis_index("sp") * group_rows + jnp.arange(group_rows, dtype=jnp.int32)
    query_heads = rms_scaled(
        jnp.dot(query_group, query_up, preferred_element_type=jnp.float32).reshape(
            group_rows, head_count, QK_DIM
        ),
        query_norm_gain,
    )
    queries = jnp.concatenate(
        [query_heads[..., :NOPE_DIM], rotate(query_heads[..., NOPE_DIM:], positions)], axis=-1
    ).astype(jnp.bfloat16)
    send_latent = jnp.concatenate([latent_group, context_latent], axis=0)
    send_rope = jnp.concatenate([rope_group, context_rope], axis=0)
    shard_rows = send_latent.shape[0]
    initial = (
        jnp.full((head_count, group_rows), -jnp.inf, jnp.float32),
        jnp.zeros((head_count, group_rows), jnp.float32),
        jnp.zeros((group_rows, head_count, VALUE_DIM), jnp.float32),
    )

    def latent_step(carried, parts, first_index):
        key_rows, value_rows = build_keys(
            parts[0], parts[1], first_index, shard_rows, group_rows, key_up, value_up, key_norm_gain
        )
        offset = key_offset(first_index, parts[0].shape[0], shard_rows, group_rows, context_lift)
        return attend_block(carried, queries, key_rows, value_rows, offset)

    result = fold_blocks(
        initial,
        (
            lax.all_gather(send_latent, "sp", axis=0, tiled=True),
            lax.all_gather(send_rope, "sp", axis=0, tiled=True),
        ),
        shard_rows,
        latent_step,
    )
    running_max, weight_sum, accumulated = result
    attended = (
        (accumulated / weight_sum.T[:, :, None])
        .reshape(group_rows, head_count * VALUE_DIM)
        .astype(jnp.bfloat16)
    )
    mixed_sum = lax.psum_scatter(
        jnp.dot(attended, out_weight, preferred_element_type=jnp.float32).astype(jnp.bfloat16),
        "tp",
        scatter_dimension=0,
        tiled=True,
    ).astype(jnp.float32)
    return (token_values + mod_gate * mixed_sum).astype(jnp.bfloat16)


def solution(mesh):
    in_specs = (
        P(("dp", "sp", "tp"), None),
        P(("dp", "sp")),
        P("sp", "tp"),
        P("sp", "tp"),
        P("sp", "tp"),
        P(),
        P(),
        P(),
        P(),
        P(),
        P(),
        P(None, "tp"),
        P(None, "tp"),
        P(None, "tp"),
        P(),
        P(),
        P("tp", None),
        P(("dp", "sp"), None),
        P(("dp", "sp"), None),
        P("tp"),
    )
    out_specs = P(("dp", "sp", "tp"), None)
    return jax.shard_map(local, mesh=mesh, in_specs=in_specs, out_specs=out_specs, check_vma=False)
```

profile of v0, /device:TPU:9, one launch (start us, length us, event | category | flops | bytes accessed | tf_op | source)
XLA Modules:
  0.0 202.2 jit_solution(5876710164665729727)
XLA Ops:
  11.1 7.9 %all-reduce = (f32[512]{0:T(512)S(1)}, f32[512]{0:T(512)S(1)}, f32[512]{0:T(512)}) all-reduce(f32[512]{0:T(512)S(1)} %bitcast.124, f32[512]{0:T(512)S(1)} %bitcast.123, f32[512]{0:T(512)S(1)} %bitcast.122), channel_id=1, replica_groups=mesh['sp'=4,'tp'=4,'dp'=2] {'sp'}, use_global_device_ids=true, to_apply=%region_3.4 | all-reduce | flops 1536 | bytes 12288 | tf_op jit(solution)/shard_map/psum | solution.py:144
  19.0 6.1 %all-gather.1 = f32[4,1,512]{2,1,0:T(1,128)S(1)} all-gather(f32[1,1,512]{2,1,0:T(1,128)S(1)} %bitcast.133), channel_id=1, replica_groups=mesh['sp'=4,'tp'=4,'dp'=2] {'tp'}, dimensions={0}, use_global_device_ids=true | all-gather | bytes 10240 | tf_op jit(solution)/shard_map/all_gather | solution.py:147
  25.1 6.0 %all-gather.2 = f32[4,1,512]{2,1,0:T(1,128)S(1)} all-gather(f32[1,1,512]{2,1,0:T(1,128)S(1)} %bitcast.132), channel_id=1, replica_groups=mesh['sp'=4,'tp'=4,'dp'=2] {'tp'}, dimensions={0}, use_global_device_ids=true | all-gather | bytes 10240 | tf_op jit(solution)/shard_map/all_gather | solution.py:146
  32.4 1.7 multiply_reduce_fusion.3
  34.2 6.0 %all_gather.27 = bf16[512,256]{1,0:T(8,128)(2,1)S(1)} all-gather(bf16[128,256]{1,0:T(8,128)(2,1)S(1)} %multiply_convert_fusion.1), channel_id=1, replica_groups=mesh['sp'=4,'tp'=4,'dp'=2] {'tp'}, dimensions={0}, use_global_device_ids=true | all-gather | bytes 327680 | tf_op jit(solution)/shard_map/all_gather | solution.py:163
  41.8 8.0 %all_gather.31 = bf16[512,512]{1,0:T(8,128)(2,1)S(1)} all-gather(bf16[128,512]{1,0:T(8,128)(2,1)S(1)} %multiply_convert_fusion), channel_id=1, replica_groups=mesh['sp'=4,'tp'=4,'dp'=2] {'tp'}, dimensions={0}, use_global_device_ids=true | all-gather | bytes 655360 | tf_op jit(solution)/shard_map/all_gather | solution.py:162
  52.7 5.7 %all_gather.29 = bf16[512,32]{0,1:T(8,128)(2,1)S(1)} all-gather(bf16[128,32]{0,1:T(8,128)(2,1)S(1)} %convolution_convert_fusion.2), channel_id=1, replica_groups=mesh['sp'=4,'tp'=4,'dp'=2] {'tp'}, dimensions={0}, use_global_device_ids=true | all-gather | bytes 40960 | tf_op jit(solution)/shard_map/all_gather | solution.py:164
  59.1 13.6 %all_gather.30 = bf16[3072,32]{0,1:T(8,128)(2,1)S(1)} all-gather(bf16[768,32]{0,1:T(8,128)(2,1)S(1)} %pad_maximum_fusion.6), channel_id=1, replica_groups=mesh['sp'=4,'tp'=4,'dp'=2] {'sp'}, dimensions={0}, use_global_device_ids=true | all-gather | bytes 245760 | tf_op jit(solution)/shard_map/all_gather | solution.py:198
  76.2 12.7 %all-gather.5.cloned.1.call-done = bf16[3072,256]{1,0:T(8,128)(2,1)} async-done(((bf16[768,256]{1,0:T(8,128)(2,1)}), bf16[3072,256]{1,0:T(8,128)(2,1)}) %all-gather.5.cloned.1.call-update) | async-done | bytes 1572880 | tf_op jit(solution)/shard_map/all_gather | solution.py:197
  88.9 64.2 %while.18 = (s32[]{:T(128)}, f32[4,512]{1,0:T(4,128)S(1)}, f32[4,512]{1,0:T(4,128)S(1)}, f32[512,4,64]{0,2,1:T(8,128)S(1)}, bf16[4,768,256]{2,1,0:T(8,128)(2,1)}...) while((s32[]{:T(128)}, f32[4,512]{1,0:T(4,128)S(1)}, ...), condition=%wide.region_11.12_spmd.clone, body=%wide.region_7.11_spmd.clone.sunk | while | flops 726175488 | bytes 56559976 | solution.py:114
  94.2 3.3 %bitcast_reduce_fusion.2 = (f32[4,512]{1,0:T(4,128)S(1)}, f32[4,768,512]{2,1,0:T(8,128)}) fusion(f32[4,768]{1,0:T(4,128)S(1)} %broadcast_select_fusion.2, bf16[512,4,96]{0,2,1:T(8,128)(2,1)S(1)} %get-tuple-element.462, bf16[768,4,32]{0,2,1:T(8,128)(2,1)S(1)} %fusion.111, bf16[768,4,64]{0,2,1:T(8,128)(2,1)S(1)} %slice.81), kind=kOutput, calls=%fused_computation.1.clone.1 | convolution fusion | flops 307886080 | bytes 7294976 | tf_op jit(solution)/shard_map/while/body/eval_jaxpr/qhd,khd->hqk/dot_general | solution.py:83
  98.9 4.1 %fusion.115 = f32[512,4,64]{0,2,1:T(8,128)S(1)} fusion(bf16[768,4,64]{0,2,1:T(8,128)(2,1)S(1)} %bitcast.109, f32[4,768,512]{2,1,0:T(8,128)} %get-tuple-element.423, f32[4,512]{1,0:T(4,128)S(1)} %get-tuple-element.454, f32[4,768]{1,0:T(4,128)S(1)} %broadcast_select_fusion.2, f32[512,4,64]{0,2,1:T(8,128)S(1)} %get-tuple-element.442, ...), kind=kOutput, calls=%fused_computation.9.clone.1 | convolution fusion | flops 208011264 | bytes 7761921 | tf_op jit(solution)/shard_map/while/body/eval_jaxpr/hqk,khd->qhd/dot_general | solution.py:91
  103.5 1.4 fusion.113
  110.2 3.3 %bitcast_reduce_fusion.2 = (f32[4,512]{1,0:T(4,128)S(1)}, f32[4,768,512]{2,1,0:T(8,128)}) fusion(f32[4,768]{1,0:T(4,128)S(1)} %broadcast_select_fusion.2, bf16[512,4,96]{0,2,1:T(8,128)(2,1)S(1)} %get-tuple-element.462, bf16[768,4,32]{0,2,1:T(8,128)(2,1)S(1)} %fusion.111, bf16[768,4,64]{0,2,1:T(8,128)(2,1)S(1)} %slice.81), kind=kOutput, calls=%fused_computation.1.clone.1 | convolution fusion | flops 307886080 | bytes 7294976 | tf_op jit(solution)/shard_map/while/body/eval_jaxpr/qhd,khd->hqk/dot_general | solution.py:83
  114.9 4.1 %fusion.115 = f32[512,4,64]{0,2,1:T(8,128)S(1)} fusion(bf16[768,4,64]{0,2,1:T(8,128)(2,1)S(1)} %bitcast.109, f32[4,768,512]{2,1,0:T(8,128)} %get-tuple-element.423, f32[4,512]{1,0:T(4,128)S(1)} %get-tuple-element.454, f32[4,768]{1,0:T(4,128)S(1)} %broadcast_select_fusion.2, f32[512,4,64]{0,2,1:T(8,128)S(1)} %get-tuple-element.442, ...), kind=kOutput, calls=%fused_computation.9.clone.1 | convolution fusion | flops 208011264 | bytes 7761921 | tf_op jit(solution)/shard_map/while/body/eval_jaxpr/hqk,khd->qhd/dot_general | solution.py:91
  119.5 1.4 fusion.113
  126.3 3.3 %bitcast_reduce_fusion.2 = (f32[4,512]{1,0:T(4,128)S(1)}, f32[4,768,512]{2,1,0:T(8,128)}) fusion(f32[4,768]{1,0:T(4,128)S(1)} %broadcast_select_fusion.2, bf16[512,4,96]{0,2,1:T(8,128)(2,1)S(1)} %get-tuple-element.462, bf16[768,4,32]{0,2,1:T(8,128)(2,1)S(1)} %fusion.111, bf16[768,4,64]{0,2,1:T(8,128)(2,1)S(1)} %slice.81), kind=kOutput, calls=%fused_computation.1.clone.1 | convolution fusion | flops 307886080 | bytes 7294976 | tf_op jit(solution)/shard_map/while/body/eval_jaxpr/qhd,khd->hqk/dot_general | solution.py:83
  130.9 4.1 %fusion.115 = f32[512,4,64]{0,2,1:T(8,128)S(1)} fusion(bf16[768,4,64]{0,2,1:T(8,128)(2,1)S(1)} %bitcast.109, f32[4,768,512]{2,1,0:T(8,128)} %get-tuple-element.423, f32[4,512]{1,0:T(4,128)S(1)} %get-tuple-element.454, f32[4,768]{1,0:T(4,128)S(1)} %broadcast_select_fusion.2, f32[512,4,64]{0,2,1:T(8,128)S(1)} %get-tuple-element.442, ...), kind=kOutput, calls=%fused_computation.9.clone.1 | convolution fusion | flops 208011264 | bytes 7761921 | tf_op jit(solution)/shard_map/while/body/eval_jaxpr/hqk,khd->qhd/dot_general | solution.py:91
  142.3 3.3 %bitcast_reduce_fusion.2 = (f32[4,512]{1,0:T(4,128)S(1)}, f32[4,768,512]{2,1,0:T(8,128)}) fusion(f32[4,768]{1,0:T(4,128)S(1)} %broadcast_select_fusion.2, bf16[512,4,96]{0,2,1:T(8,128)(2,1)S(1)} %get-tuple-element.462, bf16[768,4,32]{0,2,1:T(8,128)(2,1)S(1)} %fusion.111, bf16[768,4,64]{0,2,1:T(8,128)(2,1)S(1)} %slice.81), kind=kOutput, calls=%fused_computation.1.clone.1 | convolution fusion | flops 307886080 | bytes 7294976 | tf_op jit(solution)/shard_map/while/body/eval_jaxpr/qhd,khd->hqk/dot_general | solution.py:83
  147.0 4.1 %fusion.115 = f32[512,4,64]{0,2,1:T(8,128)S(1)} fusion(bf16[768,4,64]{0,2,1:T(8,128)(2,1)S(1)} %bitcast.109, f32[4,768,512]{2,1,0:T(8,128)} %get-tuple-element.423, f32[4,512]{1,0:T(4,128)S(1)} %get-tuple-element.454, f32[4,768]{1,0:T(4,128)S(1)} %broadcast_select_fusion.2, f32[512,4,64]{0,2,1:T(8,128)S(1)} %get-tuple-element.442, ...), kind=kOutput, calls=%fused_computation.9.clone.1 | convolution fusion | flops 208011264 | bytes 7761921 | tf_op jit(solution)/shard_map/while/body/eval_jaxpr/hqk,khd->qhd/dot_general | solution.py:91
  153.1 3.3 %convolution_convert_fusion.1 = bf16[512,2048]{1,0:T(8,128)(2,1)} fusion(bf16[512,256]{0,1:T(8,128)(2,1)S(1)} %bitcast.115, bf16[256,2048]{1,0:T(8,128)(2,1)} %param.38), kind=kOutput, calls=%fused_computation.70 | convolution fusion | flops 537919488 | bytes 3407872 | tf_op jit(solution)/shard_map/dot_general | solution.py:210
  157.1 5.8 %all-gather = f32[4,1,512]{2,1,0:T(1,128)S(1)} all-gather(f32[1,1,512]{2,1,0:T(1,128)S(1)} %bitcast.131), channel_id=1, replica_groups=mesh['sp'=4,'tp'=4,'dp'=2] {'tp'}, dimensions={0}, use_global_device_ids=true | all-gather | bytes 10240 | tf_op jit(solution)/shard_map/all_gather | solution.py:148
  162.9 30.4 %reduce-scatter.2.cloned.1.call-done = bf16[128,2048]{1,0:T(8,128)(2,1)} async-done(((bf16[512,2048]{1,0:T(8,128)(2,1)}), bf16[128,2048]{1,0:T(8,128)(2,1)}) %reduce-scatter.2.cloned.1.call-update) | async-done | bytes 524304 | tf_op jit(solution)/shard_map/reduce_scatter | solution.py:209
  193.3 2.0 fusion.47
  (190 shorter events, 46.1 us)
Async XLA Ops:
  6.5 34.5 %copy-start = (bf16[2048,512]{1,0:T(8,128)(2,1)S(1)}, bf16[2048,512]{1,0:T(8,128)(2,1)}, u32[]{:S(2)}) copy-start(bf16[2048,512]{1,0:T(8,128)(2,1)} %param.28) | copy-start | bytes 6291460
  6.5 25.8 %copy-start.3 = (bf16[128,2048]{1,0:T(8,128)(2,1)S(1)}, bf16[128,2048]{1,0:T(8,128)(2,1)}, u32[]{:S(2)}) copy-start(bf16[128,2048]{1,0:T(8,128)(2,1)} %param.22) | copy-start | bytes 1572868
  6.5 25.8 %copy-start.15 = (f32[2048]{0:T(1024)S(1)}, f32[2048]{0:T(1024)}, u32[]{:S(2)}) copy-start(f32[2048]{0:T(1024)} %param.27) | copy-start | bytes 24580
  6.5 82.4 %all-gather.5.cloned.1.call-start = ((), (), s32[]{:S(2)}) async-start(), calls=%async_computation.1 | async-start | bytes 1966080 | tf_op jit(solution)/shard_map/all_gather | solution.py:197
  8.6 25.5 %copy-start.13 = (f32[256]{0:T(256)S(1)}, f32[256]{0:T(256)}, u32[]{:S(2)}) copy-start(f32[256]{0:T(256)} %param.31) | copy-start | bytes 3076
  9.8 30.3 %copy-start.6 = (bf16[256,256]{1,0:T(8,128)(2,1)S(1)}, bf16[256,256]{1,0:T(8,128)(2,1)}, u32[]{:S(2)}) copy-start(bf16[256,256]{1,0:T(8,128)(2,1)} %param.39) | copy-start | bytes 393220
  25.1 16.0 %copy-start.10 = (f32[4,1,512]{2,1,0:T(1,128)}, f32[4,1,512]{2,1,0:T(1,128)S(1)}, u32[]{:S(2)}) copy-start(f32[4,1,512]{2,1,0:T(1,128)S(1)} %broadcast_add_fusion) | copy-start | bytes 24580
  31.1 9.9 %copy-start.9 = (f32[4,1,512]{2,1,0:T(1,128)}, f32[4,1,512]{2,1,0:T(1,128)S(1)}, u32[]{:S(2)}) copy-start(f32[4,1,512]{2,1,0:T(1,128)S(1)} %all-gather.2) | copy-start | bytes 24580
  32.4 9.3 %copy-start.17 = (f32[128]{0:T(128)}, f32[128]{0:T(128)S(1)}, u32[]{:S(2)}) copy-start(f32[128]{0:T(128)S(1)} %add_rsqrt_fusion.4) | copy-start | bytes 1540
  41.0 152.3 %reduce-scatter.2.cloned.1.call-start = ((), (), s32[]{:S(2)}) async-start(), calls=%async_computation.2 | async-start | bytes 2621440 | tf_op jit(solution)/shard_map/reduce_scatter | solution.py:209
  41.1 8.7 %copy-start.5 = (bf16[512,384]{1,0:T(8,128)(2,1)S(1)}, bf16[512,384]{1,0:T(8,128)(2,1)}, u32[]{:S(2)}) copy-start(bf16[512,384]{1,0:T(8,128)(2,1)} %param.33) | copy-start | bytes 1179652
  41.7 8.7 %copy-start.14 = (f32[96]{0:T(128)S(1)}, f32[96]{0:T(128)}, u32[]{:S(2)}) copy-start(f32[96]{0:T(128)} %param.36) | copy-start | bytes 1156
  51.3 37.6 %copy-start.2 = (bf16[256,256]{1,0:T(8,128)(2,1)S(1)}, bf16[256,256]{1,0:T(8,128)(2,1)}, u32[]{:S(2)}) copy-start(bf16[256,256]{1,0:T(8,128)(2,1)} %param.35) | copy-start | bytes 393220
  91.4 2.7 %copy-start.7 = (f32[4]{0:T(128)S(1)}, f32[4]{0:T(128)}, u32[]{:S(2)}) copy-start(f32[4]{0:T(128)} %get-tuple-element.463) | copy-start | bytes 52 | tf_op jit(solution)/shard_map/while
  98.9 4.6 %copy-start.1 = (f32[4,768,512]{2,1,0:T(8,128)S(1)}, f32[4,768,512]{2,1,0:T(8,128)}, u32[]{:S(2)}) copy-start(f32[4,768,512]{2,1,0:T(8,128)} %get-tuple-element.423) | copy-start | bytes 18874372 | tf_op jit(solution)/shard_map/while
  104.9 2.3 %copy-start.8 = (f32[96]{0:T(128)S(1)}, f32[96]{0:T(128)}, u32[]{:S(2)}) copy-start(f32[96]{0:T(128)} %get-tuple-element.460) | copy-start | bytes 1156 | tf_op jit(solution)/shard_map/while
  107.5 2.7 %copy-start.7 = (f32[4]{0:T(128)S(1)}, f32[4]{0:T(128)}, u32[]{:S(2)}) copy-start(f32[4]{0:T(128)} %get-tuple-element.463) | copy-start | bytes 52 | tf_op jit(solution)/shard_map/while
  114.9 4.6 %copy-start.1 = (f32[4,768,512]{2,1,0:T(8,128)S(1)}, f32[4,768,512]{2,1,0:T(8,128)}, u32[]{:S(2)}) copy-start(f32[4,768,512]{2,1,0:T(8,128)} %get-tuple-element.423) | copy-start | bytes 18874372 | tf_op jit(solution)/shard_map/while
  123.5 2.7 %copy-start.7 = (f32[4]{0:T(128)S(1)}, f32[4]{0:T(128)}, u32[]{:S(2)}) copy-start(f32[4]{0:T(128)} %get-tuple-element.463) | copy-start | bytes 52 | tf_op jit(solution)/shard_map/while
  130.9 4.6 %copy-start.1 = (f32[4,768,512]{2,1,0:T(8,128)S(1)}, f32[4,768,512]{2,1,0:T(8,128)}, u32[]{:S(2)}) copy-start(f32[4,768,512]{2,1,0:T(8,128)} %get-tuple-element.423) | copy-start | bytes 18874372 | tf_op jit(solution)/shard_map/while
  137.0 2.3 %copy-start.8 = (f32[96]{0:T(128)S(1)}, f32[96]{0:T(128)}, u32[]{:S(2)}) copy-start(f32[96]{0:T(128)} %get-tuple-element.460) | copy-start | bytes 1156 | tf_op jit(solution)/shard_map/while
  139.6 2.7 %copy-start.7 = (f32[4]{0:T(128)S(1)}, f32[4]{0:T(128)}, u32[]{:S(2)}) copy-start(f32[4]{0:T(128)} %get-tuple-element.463) | copy-start | bytes 52 | tf_op jit(solution)/shard_map/while
  147.0 4.6 %copy-start.1 = (f32[4,768,512]{2,1,0:T(8,128)S(1)}, f32[4,768,512]{2,1,0:T(8,128)}, u32[]{:S(2)}) copy-start(f32[4,768,512]{2,1,0:T(8,128)} %get-tuple-element.423) | copy-start | bytes 18874372 | tf_op jit(solution)/shard_map/while
  156.4 36.9 %copy-start.4 = (bf16[128,2048]{1,0:T(8,128)(2,1)S(1)}, bf16[128,2048]{1,0:T(8,128)(2,1)}, u32[]{:S(2)}) copy-start(bf16[128,2048]{1,0:T(8,128)(2,1)} %param.22) | copy-start | bytes 1572868
  (8 other events, 8.6 us)
Sparse Core Ops, SparseCore 0:
  41.1 47.7 all-gather.4
  156.6 36.6 reduce-scatter.1
where the time goes:
time: 205 us; the launch traced here: 202 us
  blocking collectives  59 us (29%)
  matrix products  51.3 us (25%)
  waiting for transfers between devices  43.1 us (21%)
  other arithmetic  25.5 us (12%)
  between operations  13.7 us (7%)
  local copies, waits for them, and re-layouts  8.86 us (4%)
    reduce_scatter x1, waiting for transfers between devices, local(): lax.psum_scatter(jnp.dot(attended, out_weight, preferred_element_type=jnp...  30.4 us
    dot_general x4, matrix products, attend_block(): jnp.einsum('hqk,khd->qhd', weights.astype(jnp.bfloat16), value_heads, pre...  16.5 us
    all_gather x1, blocking collectives, local(): lax.all_gather(send_rope, 'sp', axis=0, tiled=True)  13.6 us
    dot_general x4, matrix products, attend_block(): jnp.einsum('qhd,khd->hqk', queries, key_heads, preferred_element_type=jnp...  13.3 us
    all_gather x1, waiting for transfers between devices, local(): lax.all_gather(send_latent, 'sp', axis=0, tiled=True)  12.7 us
    all_gather x1, blocking collectives, local(): lax.all_gather(query_latent, 'tp', axis=0, tiled=True)  7.99 us
    psum x1, blocking collectives, local(): lax.psum((shift_term, scale_term, gate_term), 'sp')  7.88 us
    all_gather x1, blocking collectives, local(): lax.all_gather(scale_sum, 'tp', axis=0, tiled=True)  6.06 us
  transfers between devices with their start and end apart: 2, of which 2 were waited for; matrix products, arithmetic and copies ran while one was open for 4% of the time, Pallas kernels for 0%

commit v1 on v0

v1 whole, which is shorter than its diff:
```python
import functools

import jax
import jax.numpy as jnp
import numpy as np
from jax import lax
from jax.experimental import pallas as pl
from jax.experimental.pallas import tpu as pltpu
from jax.sharding import PartitionSpec as P

NOPE_DIM = 64
ROPE_DIM = 32
VALUE_DIM = 64
QK_DIM = 96
GRID_W = 64
LANES = 128

EPS = 1e-06
THETA = 10000.0
LOG2E = 1.4426950408889634
MESH = pl.DeviceIdType.MESH
VMEM_SPEC = pl.BlockSpec(memory_space=pltpu.VMEM)
ANY_SPEC = pl.BlockSpec(memory_space=pl.ANY)
BF16 = jnp.bfloat16
F32 = jnp.float32


def partner_order():
    return np.arange(ROPE_DIM) ^ (ROPE_DIM // 4)


def rope_spread():
    spread = np.zeros((ROPE_DIM, LANES), np.float32)
    order = partner_order()
    for j in range(ROPE_DIM):
        spread[j, NOPE_DIM + j] = 1.0
        spread[order[j], QK_DIM + j] = 1.0
    return spread


def query_spread(heads):
    spread = np.zeros((heads * QK_DIM, heads * LANES), np.float32)
    order = partner_order()
    for h in range(heads):
        for j in range(QK_DIM):
            spread[h * QK_DIM + j, h * LANES + j] = 1.0
        for j in range(ROPE_DIM):
            spread[h * QK_DIM + NOPE_DIM + order[j], h * LANES + QK_DIM + j] = 1.0
    return spread


def head_spread(heads, width):
    spread = np.zeros((heads * width, heads * LANES), np.float32)
    for h in range(heads):
        for j in range(width):
            spread[h * width + j, h * LANES + j] = 1.0
    return spread


def turn_tables(count, axis):
    freq_count = ROPE_DIM // 4
    inverse = np.float32(THETA) ** (-np.float32(4.0) * np.arange(freq_count, dtype=np.float32) / np.float32(ROPE_DIM))
    angles = np.arange(count, dtype=np.float32)[:, None] * inverse.astype(np.float32)
    cosine = np.zeros((count, LANES), np.float32)
    sine = np.zeros((count, LANES), np.float32)
    start = NOPE_DIM + axis * 2 * freq_count
    mid = start + freq_count
    cosine[:, start:mid] = np.cos(angles.astype(np.float64))
    cosine[:, mid : mid + freq_count] = np.cos(angles.astype(np.float64))
    sine[:, start:mid] = -np.sin(angles.astype(np.float64))
    sine[:, mid : mid + freq_count] = np.sin(angles.astype(np.float64))
    if axis == 0:
        cosine[:, :NOPE_DIM] = 1.0
    return cosine, sine


def norm_factor(values):
    return lax.rsqrt(jnp.mean(values * values, axis=-1, keepdims=True) + EPS)


def front_kernel(
    sp, tp,
    cond_ref, shift_w, scale_w, gate_w, tokens_ref, gain_ref, qd_ref, qg_ref, kd_ref, kg_ref, rd_ref,
    cl_ref, cr_ref, spread_ref,
    q_out, kv_out, ctx_out, gate_out,
    mods, q_own, kv_own, ctx_own,
    mod_send, mod_recv, q_send, q_recv, kv_send, kv_recv, c_send, c_recv, local_sem,
):
    s_me = lax.axis_index("sp")
    t_me = lax.axis_index("tp")
    me = s_me * tp + t_me
    half = mods.shape[2]
    rank = cl_ref.shape[1]

    def peer(ds, dt):
        return lax.rem(s_me + ds, sp), lax.rem(t_me + dt, tp)

    others = [(ds, dt) for ds in range(sp) for dt in range(tp) if ds or dt]
    barrier = pltpu.get_barrier_semaphore()
    for ds, dt in others:
        ps, pt = peer(ds, dt)
        pl.semaphore_signal(barrier, inc=1, device_id={"sp": ps, "tp": pt}, device_id_type=MESH)

    c = cond_ref[...].astype(F32)
    act = (c / (1.0 + jnp.exp(-c))).astype(BF16)
    act = jnp.broadcast_to(act, (16, act.shape[1]))
    rows = []
    for w in (shift_w, scale_w, gate_w):
        term = jnp.dot(act, w[...], preferred_element_type=F32)[0:1]
        rows += [term[:, :half], term[:, half:]]
    mods[me] = jnp.concatenate(rows + [rows[0], rows[0]], axis=0)

    spread = spread_ref[...]
    ctx_own[:, :rank] = cl_ref[...]
    ctx_own[:, rank:] = jnp.dot(cr_ref[...], spread, preferred_element_type=F32).astype(BF16)

    pl.semaphore_wait(barrier, len(others))
    copies = []
    mod_copies = []
    for i, (ds, dt) in enumerate(others):
        ps, pt = peer(ds, dt)
        cp = pltpu.make_async_remote_copy(
            src_ref=mods.at[me], dst_ref=mods.at[me], send_sem=mod_send.at[i], recv_sem=mod_recv.at[i],
            device_id={"sp": ps, "tp": pt}, device_id_type=MESH,
        )
        cp.start()
        mod_copies.append(cp)
    for ds in range(1, sp):
        ps, pt = peer(ds, 0)
        cp = pltpu.make_async_remote_copy(
            src_ref=ctx_own, dst_ref=ctx_out.at[s_me], send_sem=c_send.at[ds - 1], recv_sem=c_recv.at[ds - 1],
            device_id={"sp": ps, "tp": pt}, device_id_type=MESH,
        )
        cp.start()
        copies.append(cp)
    own = [pltpu.make_async_copy(ctx_own, ctx_out.at[s_me], local_sem.at[0])]
    own[0].start()

    x = tokens_ref[...].astype(F32)
    xn = x * norm_factor(x) * gain_ref[...]

    for cp in mod_copies:
        cp.wait_recv()
    pieces = [[], [], []]
    for t in range(tp):
        total = mods[t]
        for s in range(1, sp):
            total = total + mods[s * tp + t]
        for k in range(3):
            pieces[k] += [total[2 * k : 2 * k + 1], total[2 * k + 1 : 2 * k + 2]]
    shift, scale, gate = [jnp.concatenate(p, axis=1) for p in pieces]
    gate_out[...] = gate
    normed = (xn * (1.0 + scale) + shift).astype(BF16)

    q = jnp.dot(normed, qd_ref[...], preferred_element_type=F32)
    q_own[...] = (q * norm_factor(q) * qg_ref[...]).astype(BF16)
    kv = jnp.dot(normed, kd_ref[...], preferred_element_type=F32)
    kv_own[:, :rank] = (kv * norm_factor(kv) * kg_ref[...]).astype(BF16)
    rope = jnp.dot(normed, rd_ref[...], preferred_element_type=F32).astype(BF16)
    kv_own[:, rank:] = jnp.dot(rope, spread, preferred_element_type=F32).astype(BF16)

    for dt in range(1, tp):
        ps, pt = peer(0, dt)
        cp = pltpu.make_async_remote_copy(
            src_ref=q_own, dst_ref=q_out.at[t_me], send_sem=q_send.at[dt - 1], recv_sem=q_recv.at[dt - 1],
            device_id={"sp": ps, "tp": pt}, device_id_type=MESH,
        )
        cp.start()
        copies.append(cp)
    for i, (ds, dt) in enumerate(others):
        ps, pt = peer(ds, dt)
        cp = pltpu.make_async_remote_copy(
            src_ref=kv_own, dst_ref=kv_out.at[me], send_sem=kv_send.at[i], recv_sem=kv_recv.at[i],
            device_id={"sp": ps, "tp": pt}, device_id_type=MESH,
        )
        cp.start()
        copies.append(cp)
    own.append(pltpu.make_async_copy(q_own, q_out.at[t_me], local_sem.at[1]))
    own.append(pltpu.make_async_copy(kv_own, kv_out.at[me], local_sem.at[2]))
    own[1].start()
    own[2].start()
    for cp in mod_copies:
        cp.wait_send()
    for cp in copies:
        cp.wait()
    for cp in own:
        cp.wait()


def attend_kernel(
    heads, s_ref, q_ref, kv_ref, ctx_ref, qu_ref, ku_ref, vu_ref, qe_ref, ke_ref, ve_ref,
    qgain_ref, kgain_ref, lift_ref, row_a, row_b, col_a, col_b, out_ref,
    k_lat, v_lat, k_ctx, v_ctx, q_all,
):
    rank = ku_ref.shape[0]
    tokens = kv_ref.shape[0]
    group = q_ref.shape[0]
    context = ctx_ref.shape[0]
    lane = lax.broadcasted_iota(jnp.int32, (1, LANES), 1)
    live = lane < QK_DIM
    ones_lane = jnp.where(lane == VALUE_DIM, 1.0, 0.0).astype(F32)
    qu = jnp.dot(qu_ref[...], qe_ref[...], preferred_element_type=F32).astype(BF16)
    ku = jnp.dot(ku_ref[...], ke_ref[...], preferred_element_type=F32).astype(BF16)
    vu = jnp.dot(vu_ref[...], ve_ref[...], preferred_element_type=F32).astype(BF16)

    def tables(first_row, row_count, gain):
        gain_partner = pltpu.roll(gain, QK_DIM, 1)
        a = [(row_a[pl.ds(first_row + r, 1), :] + col_a[...]) * gain[0:1] for r in range(row_count)]
        b = [(row_b[pl.ds(first_row + r, 1), :] + col_b[...]) * gain_partner[0:1] for r in range(row_count)]
        return jnp.concatenate(a, axis=0), jnp.concatenate(b, axis=0)

    def finish(v, a, b):
        square = jnp.where(live, v * v, 0.0)
        factor = lax.rsqrt(jnp.sum(square, axis=-1, keepdims=True) * (1.0 / QK_DIM) + EPS)
        if b is None:
            return (v * a * factor).astype(BF16)
        return ((v * a + pltpu.roll(v, QK_DIM, 1) * b) * factor).astype(BF16)

    block = min(256, group)
    grid_rows = block // GRID_W
    qgain = qgain_ref[...]
    kgain = kgain_ref[...]

    def query_block(i, carry):
        start = pl.multiple_of(i * block, block)
        q = jnp.dot(q_ref[pl.ds(start, block), :], qu, preferred_element_type=F32)
        a, b = tables(s_ref[0] * (group // GRID_W) + i * grid_rows, grid_rows, qgain)
        for h in range(heads):
            q_all[h, pl.ds(start, block), :] = finish(q[:, h * LANES : (h + 1) * LANES], a, b)
        return carry

    lax.fori_loop(0, group // block, query_block, 0)

    def key_block(i, carry):
        start = pl.multiple_of(i * block, block)
        lat = kv_ref[pl.ds(start, block), :rank]
        rope = kv_ref[pl.ds(start, block), rank:].astype(F32)
        k = jnp.dot(lat, ku, preferred_element_type=F32)
        v = jnp.dot(lat, vu, preferred_element_type=F32)
        a, b = tables(i * grid_rows, grid_rows, kgain)
        for h in range(heads):
            k_lat[h, pl.ds(start, block), :] = finish(k[:, h * LANES : (h + 1) * LANES] + rope, a, b)
            v_lat[h, pl.ds(start, block), :] = (v[:, h * LANES : (h + 1) * LANES] + ones_lane).astype(BF16)
        return carry

    lax.fori_loop(0, tokens // block, key_block, 0)
    plain = jnp.where(live, kgain[0:1], 0.0)

    def context_block(i, carry):
        start = pl.multiple_of(i * block, block)
        lat = ctx_ref[pl.ds(start, block), :rank]
        rope = ctx_ref[pl.ds(start, block), rank:].astype(F32)
        k = jnp.dot(lat, ku, preferred_element_type=F32)
        v = jnp.dot(lat, vu, preferred_element_type=F32)
        for h in range(heads):
            k_ctx[h, pl.ds(start, block), :] = finish(k[:, h * LANES : (h + 1) * LANES] + rope, plain, None)
            v_ctx[h, pl.ds(start, block), :] = (v[:, h * LANES : (h + 1) * LANES] + ones_lane).astype(BF16)
        return carry

    lax.fori_loop(0, context // block, context_block, 0)

    factor = LOG2E * QK_DIM ** (-0.5)
    contract = (((1,), (1,)), ((), ()))
    q_rows = min(256, group)

    def attend(i, carry):
        start = pl.multiple_of(i * q_rows, q_rows)
        outs = []
        for h in range(heads):
            q = q_all[h, pl.ds(start, q_rows), :]
            s_lat = lax.dot_general(q, k_lat[h], contract, preferred_element_type=F32)
            s_ctx = lax.dot_general(q, k_ctx[h], contract, preferred_element_type=F32)
            lift = lift_ref[h] * LOG2E
            top = jnp.maximum(
                jnp.max(s_lat, axis=-1, keepdims=True) * factor,
                jnp.max(s_ctx, axis=-1, keepdims=True) * factor + lift,
            )
            p_lat = jnp.exp2(s_lat * factor - top).astype(BF16)
            p_ctx = jnp.exp2(s_ctx * factor - (top - lift)).astype(BF16)
            acc = jnp.dot(p_lat, v_lat[h], preferred_element_type=F32) + jnp.dot(
                p_ctx, v_ctx[h], preferred_element_type=F32
            )
            outs.append((acc[:, :VALUE_DIM] / acc[:, VALUE_DIM : VALUE_DIM + 1]).astype(BF16))
        out_ref[pl.ds(start, q_rows), :] = jnp.concatenate(outs, axis=1)
        return carry

    lax.fori_loop(0, group // q_rows, attend, 0)


def tail_kernel(tp, att_ref, tokens_ref, gate_ref, *rest):
    weights = rest[:tp]
    out_ref, held, send_sem, recv_sem = rest[tp:]
    t_me = lax.axis_index("tp")
    rows = tokens_ref.shape[0]
    barrier = pltpu.get_barrier_semaphore()
    for dt in range(1, tp):
        pl.semaphore_signal(barrier, inc=1, device_id={"tp": lax.rem(t_me + dt, tp)}, device_id_type=MESH)
    pl.semaphore_wait(barrier, tp - 1)
    copies = []
    for dt in range(1, tp):
        dest = lax.rem(t_me + dt, tp)
        cp = pltpu.make_async_remote_copy(
            src_ref=att_ref.at[dest], dst_ref=held.at[dt - 1],
            send_sem=send_sem.at[dt - 1], recv_sem=recv_sem.at[dt - 1],
            device_id={"tp": dest}, device_id_type=MESH,
        )
        cp.start()
        copies.append(cp)
    chunk = 512
    width = out_ref.shape[1]
    gate = gate_ref[...]
    for dt in range(1, tp):
        copies[dt - 1].wait()
    for n in range(width // chunk):
        cols = slice(n * chunk, (n + 1) * chunk)
        mixed = jnp.dot(att_ref[t_me], weights[0][:, cols], preferred_element_type=F32).astype(BF16).astype(F32)
        for dt in range(1, tp):
            mixed = mixed + jnp.dot(
                held[dt - 1], weights[dt][:, cols], preferred_element_type=F32
            ).astype(BF16).astype(F32)
        out_ref[:, cols] = (tokens_ref[:, cols].astype(F32) + gate[:, cols] * mixed).astype(BF16)


def local(
    sp, tp, dp,
    latent_tokens, condition, shift_weight, scale_weight, gate_weight, norm_gain,
    query_down, query_gain, kv_down, kv_gain, rope_down, query_up, key_up, value_up,
    query_norm_gain, key_norm_gain, out_weight, context_latent, context_rope, context_lift,
):
    rows, width = latent_tokens.shape
    q_rank = query_down.shape[1]
    rank = kv_down.shape[1]
    heads = query_up.shape[1] // QK_DIM
    ctx_rows = context_latent.shape[0]
    group = rows * tp
    tokens = group * sp
    n_dev = sp * tp

    k_rows = out_weight.shape[0]
    half = k_rows // dp
    d_me = lax.axis_index("dp")
    mine = lax.dynamic_slice_in_dim(out_weight, d_me * half, half, axis=0)
    weights = [out_weight]
    for dt in range(1, tp):
        got = lax.ppermute(mine, "tp", [(i, (i + dt) % tp) for i in range(tp)])
        other = lax.ppermute(got, "dp", [(i, (i + 1) % dp) for i in range(dp)])
        weights.append((got, other))

    front = pl.pallas_call(
        functools.partial(front_kernel, sp, tp),
        out_shape=(
            jax.ShapeDtypeStruct((tp, rows, q_rank), BF16),
            jax.ShapeDtypeStruct((n_dev, rows, rank + LANES), BF16),
            jax.ShapeDtypeStruct((sp, ctx_rows, rank + LANES), BF16),
            jax.ShapeDtypeStruct((1, width), F32),
        ),
        in_specs=[VMEM_SPEC] * 14,
        out_specs=(ANY_SPEC, ANY_SPEC, ANY_SPEC, VMEM_SPEC),
        scratch_shapes=[
            pltpu.VMEM((n_dev, 8, width // tp // 2), F32),
            pltpu.VMEM((rows, q_rank), BF16),
            pltpu.VMEM((rows, rank + LANES), BF16),
            pltpu.VMEM((ctx_rows, rank + LANES), BF16),
            pltpu.SemaphoreType.DMA((n_dev - 1,)),
            pltpu.SemaphoreType.DMA((n_dev - 1,)),
            pltpu.SemaphoreType.DMA((tp - 1,)),
            pltpu.SemaphoreType.DMA((tp - 1,)),
            pltpu.SemaphoreType.DMA((n_dev - 1,)),
            pltpu.SemaphoreType.DMA((n_dev - 1,)),
            pltpu.SemaphoreType.DMA((sp - 1,)),
            pltpu.SemaphoreType.DMA((sp - 1,)),
            pltpu.SemaphoreType.DMA((3,)),
        ],
        compiler_params=pltpu.CompilerParams(
            collective_id=0, has_side_effects=True, vmem_limit_bytes=32 * 1024 * 1024
        ),
        cost_estimate=pl.CostEstimate(flops=20_000_000_000, bytes_accessed=8_000_000, transcendentals=0),
        name="front",
    )
    q_group, kv_all, ctx_all, mod_gate = front(
        condition[None], shift_weight, scale_weight, gate_weight, latent_tokens, norm_gain[None],
        query_down, query_gain[None], kv_down, kv_gain[None], rope_down,
        context_latent, context_rope, jnp.asarray(rope_spread(), BF16),
    )

    def extended(gain):
        freq = ROPE_DIM // 4
        parts = [gain]
        for axis in range(2):
            start = NOPE_DIM + axis * 2 * freq
            parts += [gain[start + freq : start + 2 * freq], gain[start : start + freq]]
        return jnp.broadcast_to(jnp.concatenate(parts)[None], (8, LANES))

    row_a, row_b = turn_tables(tokens // GRID_W, 0)
    col_a, col_b = turn_tables(GRID_W, 1)
    context = sp * ctx_rows
    smem = pl.BlockSpec(memory_space=pltpu.SMEM)
    attended = pl.pallas_call(
        functools.partial(attend_kernel, heads),
        out_shape=jax.ShapeDtypeStruct((group, heads * VALUE_DIM), BF16),
        in_specs=[smem] + [VMEM_SPEC] * 11 + [smem] + [VMEM_SPEC] * 4,
        out_specs=VMEM_SPEC,
        scratch_shapes=[
            pltpu.VMEM((heads, tokens, LANES), BF16),
            pltpu.VMEM((heads, tokens, LANES), BF16),
            pltpu.VMEM((heads, context, LANES), BF16),
            pltpu.VMEM((heads, context, LANES), BF16),
            pltpu.VMEM((heads, group, LANES), BF16),
        ],
        compiler_params=pltpu.CompilerParams(vmem_limit_bytes=60 * 1024 * 1024),
        cost_estimate=pl.CostEstimate(flops=20_000_000_000, bytes_accessed=8_000_000, transcendentals=0),
        name="attend",
    )(
        lax.axis_index("sp").astype(jnp.int32)[None],
        q_group.reshape(group, q_rank), kv_all.reshape(tokens, rank + LANES),
        ctx_all.reshape(context, rank + LANES), query_up, key_up, value_up,
        jnp.asarray(query_spread(heads), BF16), jnp.asarray(head_spread(heads, NOPE_DIM), BF16),
        jnp.asarray(head_spread(heads, VALUE_DIM), BF16),
        extended(query_norm_gain), extended(key_norm_gain), context_lift,
        jnp.asarray(row_a), jnp.asarray(row_b), jnp.asarray(col_a), jnp.asarray(col_b),
    )

    full = [out_weight]
    for got, other in weights[1:]:
        low = jnp.where(d_me == 0, got, other)
        high = jnp.where(d_me == 0, other, got)
        full.append(jnp.concatenate([low, high], axis=0))
    return pl.pallas_call(
        functools.partial(tail_kernel, tp),
        out_shape=jax.ShapeDtypeStruct((rows, width), BF16),
        in_specs=[VMEM_SPEC] * (3 + tp),
        out_specs=VMEM_SPEC,
        scratch_shapes=[
            pltpu.VMEM((tp - 1, rows, heads * VALUE_DIM), BF16),
            pltpu.SemaphoreType.DMA((tp - 1,)),
            pltpu.SemaphoreType.DMA((tp - 1,)),
        ],
        compiler_params=pltpu.CompilerParams(
            collective_id=1, has_side_effects=True, vmem_limit_bytes=32 * 1024 * 1024
        ),
        name="tail",
    )(attended.reshape(tp, rows, heads * VALUE_DIM), latent_tokens, mod_gate, *full)


def solution(mesh):
    in_specs = (
        P(("dp", "sp", "tp"), None), P(("dp", "sp")), P("sp", "tp"), P("sp", "tp"), P("sp", "tp"),
        P(), P(), P(), P(), P(), P(), P(None, "tp"), P(None, "tp"), P(None, "tp"), P(), P(),
        P("tp", None), P(("dp", "sp"), None), P(("dp", "sp"), None), P("tp"),
    )
    out_specs = P(("dp", "sp", "tp"), None)
    body = functools.partial(local, mesh.shape["sp"], mesh.shape["tp"], mesh.shape["dp"])
    return jax.shard_map(body, mesh=mesh, in_specs=in_specs, out_specs=out_specs, check_vma=False)
```

time: 205 us -> 120 us (0.59)
  Pallas kernels: 0 us -> 92.6 us
  blocking collectives: 59 us -> 0 us
  matrix products: 51.3 us -> 0 us
  waiting for transfers between devices: 43.1 us -> 1.13 us
  other arithmetic: 25.5 us -> 0.49 us
  between operations: 13.7 us -> 0.15 us
  local copies, waits for them, and re-layouts: 8.86 us -> 19.7 us
  starting transfers between devices: 0.04 us -> 4.98 us
    pallas_call x0 -> x3, Pallas kernels: none -> 92.6 us  [the longest x1 58.4 us: local(): front(condition[None], shift_weight, scale_weight, gate_weight, latent_to...]
    dot_general x24 -> x0, matrix products: 51.3 us -> none  [the longest x4 16.5 us: attend_block(): jnp.einsum('hqk,khd->qhd', weights.astype(jnp.bfloat16), value_heads, pre...]
    all_gather x7 -> x0, blocking collectives: 51.2 us -> none  [the longest x1 13.6 us: local(): lax.all_gather(send_rope, 'sp', axis=0, tiled=True)]
    reduce_scatter x1 -> x0, waiting for transfers between devices: 30.4 us -> none  [local(): lax.psum_scatter(jnp.dot(attended, out_weight, preferred_element_type=jnp...]
    unnamed x29 -> x41, local copies, waits for them, and re-layouts: 1.7 us -> 16.4 us
    all_gather x1 -> x0, waiting for transfers between devices: 12.7 us -> none  [local(): lax.all_gather(send_latent, 'sp', axis=0, tiled=True)]
    convert_element_type x14 -> x0, other arithmetic: 9.01 us -> none  [the longest x4 3.25 us: build_keys(): rope_rows.astype(jnp.float32)[:, None, :]]
    psum x1 -> x0, blocking collectives: 7.88 us -> none  [local(): lax.psum((shift_term, scale_term, gate_term), 'sp')]
  transfers between devices with their start and end apart: 2 -> 6, of which waited for: 2 -> 1; matrix products, arithmetic and copies ran while one was open for 4% -> 4% of each run, Pallas kernels for 0% -> 71%
where the time goes in v1:
time: 120 us; the launch traced here: 119 us
  Pallas kernels  92.6 us (77%)
  local copies, waits for them, and re-layouts  19.7 us (16%)
  starting transfers between devices  4.98 us (4%)
    pallas_call x1, Pallas kernels, local(): front(condition[None], shift_weight, scale_weight, gate_weight, latent_to...  58.4 us
    pallas_call x1, Pallas kernels, local(): pl.pallas_call(functools.partial(attend_kernel, heads), out_shape=jax.Sha...  26 us
    unnamed x41, local copies, waits for them, and re-layouts  16.4 us
    pallas_call x1, Pallas kernels, local(): pl.pallas_call(functools.partial(tail_kernel, tp), out_shape=jax.ShapeDty...  8.25 us
    ppermute x3, starting transfers between devices, local(): got = lax.ppermute(mine, 'tp', [(i, (i + dt) % tp) for i in range(tp)])  3.66 us
  transfers between devices with their start and end apart: 6, of which 1 were waited for; matrix products, arithmetic and copies ran while one was open for 4% of the time, Pallas kernels for 71%

profile of v1, /device:TPU:9, one launch (start us, length us, event | category | flops | bytes accessed | tf_op | source)
XLA Modules:
  0.0 119.1 jit_solution(4250906559390171165)
XLA Ops:
  0.0 1.1 constant_dynamic-slice_fusion
  1.1 1.3 %collective-permute-start = (bf16[128,2048]{1,0:T(8,128)(2,1)S(1)}, bf16[128,2048]{1,0:T(8,128)(2,1)S(1)}, u32[]{:S(2)}, u32[]{:S(2)}) collective-permute-start(bf16[128,2048]{1,0:T(8,128)(2,1)S(1)} %constant_dynamic-slice_fusion), channel_id=1, source_target_pairs={{0,2},{2,4},{4,6},{6,0},{1,3},{3,5},{5,7},{7,1},{8,10},{10,12},{12... | collective-permute-start | bytes 1572872 | tf_op jit(solution)/shard_map/ppermute | solution.py:345
  2.4 1.2 %collective-permute-start.2 = (bf16[128,2048]{1,0:T(8,128)(2,1)S(1)}, bf16[128,2048]{1,0:T(8,128)(2,1)S(1)}, u32[]{:S(2)}, u32[]{:S(2)}) collective-permute-start(bf16[128,2048]{1,0:T(8,128)(2,1)S(1)} %constant_dynamic-slice_fusion), channel_id=1, source_target_pairs={{0,4},{2,6},{4,0},{6,2},{1,5},{3,7},{5,1},{7,3},{8,12},{10,14},{12... | collective-permute-start | bytes 1572872 | tf_op jit(solution)/shard_map/ppermute | solution.py:345
  3.6 1.2 collective-permute-start.4
  5.4 1.2 copy.29.rd_ref
  6.6 0.8 copy.30.cr_ref
  7.5 1.0 copy-done.1
  8.5 1.6 %copy-done.4 = bf16[2048,512]{1,0:T(8,128)(2,1)S(1)} copy-done((bf16[2048,512]{1,0:T(8,128)(2,1)S(1)}, bf16[2048,512]{1,0:T(8,128)(2,1)}, u32[]{:S(2)}) %copy-start.4) | copy-done | bytes 2097176
  10.1 1.2 %copy-done.5 = bf16[2048,256]{1,0:T(8,128)(2,1)S(1)} copy-done((bf16[2048,256]{1,0:T(8,128)(2,1)S(1)}, bf16[2048,256]{1,0:T(8,128)(2,1)}, u32[]{:S(2)}) %copy-start.5) | copy-done | bytes 1048600
  11.3 1.0 copy-done.6
  12.4 1.0 copy-done.7
  13.4 1.0 copy-done.8
  14.4 0.9 copy-done.9
  15.3 0.7 copy-done.10
  17.4 0.7 copy-done.16
  18.1 58.4 %front.1 = (bf16[4,128,512]{2,1,0:T(8,128)(2,1)S(1)}, bf16[16,128,384]{2,1,0:T(8,128)(2,1)S(1)}, bf16[4,256,384]{2,1,0:T(8,128)(2,1)S(1)}, f32[1,2048]{1,0:T(1,128)S(1)}) custom-call(bf16[1,512]{1,0:T(2,128)(2,1)S(1)} %broadcast_in_dim.28.cond_ref, bf16[512,512]{1,0:T(8,128)(2,1)S(1)} %copy-done.6, bf16[512,512]{1,0:T(8,128)(2,1)S(1)} %copy-done.7, ...), custom_call_target="tpu_custom_call" | custom-call | flops 20000000000 | bytes 8000000 | tf_op jit(solution)/shard_map/front/pallas_call | solution.py:380
  76.5 1.2 copy-done.13
  77.7 0.9 copy-done.14
  78.6 0.8 copy-done.15
  79.7 0.8 collective-permute-start.1
  81.8 26.0 %attend.1 = bf16[512,256]{1,0:T(8,128)(2,1)} custom-call(s32[1]{0:T(128)} %bitcast.s_ref, bf16[512,512]{1,0:T(8,128)(2,1)} %bitcast.14, bf16[2048,384]{1,0:T(8,128)(2,1)} %bitcast.12, bf16[1024,384]{1,0:T(8,128)(2,1)} %bitcast.13, bf16[512,384]{1,0:T(8,128)(2,1)} %qu_ref.1, bf16[256,256]{1,0:T(8,128)(2,1)} %ku_ref.1, bf16[256,256]{1,0:T(8,128)(2,1)} %vu_ref.1, ...), custom_call_target="tpu_custom_call" | custom-call | flops 20000000000 | bytes 8000000 | tf_op jit(solution)/shard_map/attend/pallas_call | solution.py:398
  108.6 1.1 collective-permute-done.5
  110.0 8.2 %tail.1 = bf16[128,2048]{1,0:T(8,128)(2,1)S(1)} custom-call(bf16[4,128,256]{2,1,0:T(8,128)(2,1)S(1)} %bitcast.8, bf16[128,2048]{1,0:T(8,128)(2,1)S(1)} %copy-done.2, f32[1,2048]{1,0:T(1,128)S(1)} %get-tuple-element.12.gate_ref, bf16[256,2048]{1,0:T(8,128)(2,1)S(1)} %copy-done, bf16[256,2048]{1,0:T(8,128)(2,1)S(1)} %pad_maximum_fusion.rest_1_, ...), custom_call_target="tpu_custom_call" | custom-call | tf_op jit(solution)/shard_map/tail/pallas_call | solution.py:428
  118.3 0.8 copy.32
  (46 shorter events, 4.8 us)
Async XLA Ops:
  1.1 78.7 %collective-permute-start = (bf16[128,2048]{1,0:T(8,128)(2,1)S(1)}, bf16[128,2048]{1,0:T(8,128)(2,1)S(1)}, u32[]{:S(2)}, u32[]{:S(2)}) collective-permute-start(bf16[128,2048]{1,0:T(8,128)(2,1)S(1)} %constant_dynamic-slice_fusion), channel_id=1, source_target_pairs={{0,2},{2,4},{4,6},{6,0},{1,3},{3,5},{5,7},{7,1},{8,10},{10,12},{12... | collective-permute-start | bytes 1572872 | tf_op jit(solution)/shard_map/ppermute | solution.py:345
  2.4 78.2 %collective-permute-start.2 = (bf16[128,2048]{1,0:T(8,128)(2,1)S(1)}, bf16[128,2048]{1,0:T(8,128)(2,1)S(1)}, u32[]{:S(2)}, u32[]{:S(2)}) collective-permute-start(bf16[128,2048]{1,0:T(8,128)(2,1)S(1)} %constant_dynamic-slice_fusion), channel_id=1, source_target_pairs={{0,4},{2,6},{4,0},{6,2},{1,5},{3,7},{5,1},{7,3},{8,12},{10,14},{12... | collective-permute-start | bytes 1572872 | tf_op jit(solution)/shard_map/ppermute | solution.py:345
  3.6 104.1 %collective-permute-start.4 = (bf16[128,2048]{1,0:T(8,128)(2,1)S(1)}, bf16[128,2048]{1,0:T(8,128)(2,1)S(1)}, u32[]{:S(2)}, u32[]{:S(2)}) collective-permute-start(bf16[128,2048]{1,0:T(8,128)(2,1)S(1)} %constant_dynamic-slice_fusion), channel_id=1, source_target_pairs={{0,6},{2,0},{4,2},{6,4},{1,7},{3,1},{5,3},{7,5},{8,14},{10,8},{12,... | collective-permute-start | bytes 1572872 | tf_op jit(solution)/shard_map/ppermute | solution.py:345
  7.4 1.0 copy-start.1
  8.5 1.6 %copy-start.4 = (bf16[2048,512]{1,0:T(8,128)(2,1)S(1)}, bf16[2048,512]{1,0:T(8,128)(2,1)}, u32[]{:S(2)}) copy-start(bf16[2048,512]{1,0:T(8,128)(2,1)} %qd_ref.1) | copy-start | bytes 6291460
  10.1 1.2 %copy-start.5 = (bf16[2048,256]{1,0:T(8,128)(2,1)S(1)}, bf16[2048,256]{1,0:T(8,128)(2,1)}, u32[]{:S(2)}) copy-start(bf16[2048,256]{1,0:T(8,128)(2,1)} %kd_ref.1) | copy-start | bytes 3145732
  11.3 1.0 copy-start.6
  12.4 1.0 copy-start.7
  13.4 1.0 copy-start.8
  14.4 0.9 copy-start.9
  15.3 0.7 copy-start.10
  16.0 0.7 copy-start.11
  17.4 0.7 copy-start.16
  18.1 61.3 %copy-start.17 = (f32[96]{0:T(128)S(1)}, f32[96]{0:T(128)}, u32[]{:S(2)}) copy-start(f32[96]{0:T(128)} %param.42) | copy-start | bytes 1156
  18.1 61.5 %copy-start.18 = (f32[96]{0:T(128)S(1)}, f32[96]{0:T(128)}, u32[]{:S(2)}) copy-start(f32[96]{0:T(128)} %param.43) | copy-start | bytes 1156
  76.5 1.2 %copy-start.13 = (bf16[16,128,384]{2,1,0:T(8,128)(2,1)}, bf16[16,128,384]{2,1,0:T(8,128)(2,1)S(1)}, u32[]{:S(2)}) copy-start(bf16[16,128,384]{2,1,0:T(8,128)(2,1)S(1)} %get-tuple-element.10) | copy-start | bytes 4718596
  77.7 0.9 copy-start.14
  78.6 0.8 copy-start.15
  79.7 28.5 %collective-permute-start.1 = (bf16[128,2048]{1,0:T(8,128)(2,1)S(1)}, bf16[128,2048]{1,0:T(8,128)(2,1)S(1)}, u32[]{:S(2)}, u32[]{:S(2)}) collective-permute-start(bf16[128,2048]{1,0:T(8,128)(2,1)S(1)} %collective-permute-done), channel_id=1, source_target_pairs={{0,1},{1,0},{2,3},{3,2},{4,5},{5,4},{6,7},{7,6},{8,9},{9,8},{10,11... | collective-permute-start | bytes 1572872 | tf_op jit(solution)/shard_map/ppermute | solution.py:346
  80.5 27.8 %collective-permute-start.3 = (bf16[128,2048]{1,0:T(8,128)(2,1)S(1)}, bf16[128,2048]{1,0:T(8,128)(2,1)S(1)}, u32[]{:S(2)}, u32[]{:S(2)}) collective-permute-start(bf16[128,2048]{1,0:T(8,128)(2,1)S(1)} %collective-permute-done.2), channel_id=1, source_target_pairs={{0,1},{1,0},{2,3},{3,2},{4,5},{5,4},{6,7},{7,6},{8,9},{9,8},{10,11... | collective-permute-start | bytes 1572872 | tf_op jit(solution)/shard_map/ppermute | solution.py:346
  107.7 2.0 %collective-permute-start.5 = (bf16[128,2048]{1,0:T(8,128)(2,1)S(1)}, bf16[128,2048]{1,0:T(8,128)(2,1)S(1)}, u32[]{:S(2)}, u32[]{:S(2)}) collective-permute-start(bf16[128,2048]{1,0:T(8,128)(2,1)S(1)} %collective-permute-done.4), channel_id=1, source_target_pairs={{0,1},{1,0},{2,3},{3,2},{4,5},{5,4},{6,7},{7,6},{8,9},{9,8},{10,11... | collective-permute-start | bytes 1572872 | tf_op jit(solution)/shard_map/ppermute | solution.py:346
  108.6 1.3 %copy-start = (bf16[256,2048]{1,0:T(8,128)(2,1)S(1)}, bf16[256,2048]{1,0:T(8,128)(2,1)}, u32[]{:S(2)}) copy-start(bf16[256,2048]{1,0:T(8,128)(2,1)} %rest_0_.1) | copy-start | bytes 3145732
  108.6 1.3 %copy-start.2 = (bf16[128,2048]{1,0:T(8,128)(2,1)S(1)}, bf16[128,2048]{1,0:T(8,128)(2,1)}, u32[]{:S(2)}) copy-start(bf16[128,2048]{1,0:T(8,128)(2,1)} %tokens_ref.3) | copy-start | bytes 1572868
  108.6 1.4 %copy-start.3 = (bf16[512,256]{1,0:T(8,128)(2,1)S(1)}, bf16[512,256]{1,0:T(8,128)(2,1)}, u32[]{:S(2)}) copy-start(bf16[512,256]{1,0:T(8,128)(2,1)} %attend.1) | copy-start | bytes 786436
  (1 other events, 0.7 us)
